TPU v7x, 32 devices: a whole 2x2x4 slice. The times are simulated.
32 devices in a mesh: sp: 16 (over z, y, core), tp: 2 (over x).
Axes of the slice: x: 2, y: 2, z: 4, core: 2. Of those that a mesh axis runs over, the one named last changes fastest.
Arguments:
- glu_value: bfloat16 [8192, 1024], P('sp', 'tp'), may hold values from -6 to 6
- glu_gate: bfloat16 [8192, 1024], P('sp', 'tp'), may hold values from -8 to 8
- conv_taps: float32 [31, 1024], P(None, 'tp'), may hold values from -1 to 1
- channel_norm_gain: float32 [1024], P('tp'), may hold values from 0.1 to 1.9
- channel_norm_bias: float32 [1024], P('tp'), may hold values from -3 to 3
- out_proj: bfloat16 [1024, 2048], P('tp'), may hold values from -0.1875 to 0.1875
- out_grad: bfloat16 [8192, 2048], P('sp'), may hold values from -6 to 6
Outputs:
- grad_value: bfloat16 [8192, 1024], P('sp', 'tp')
- grad_gate: bfloat16 [8192, 1024], P('sp', 'tp')
- grad_taps: float32 [31, 1024], P(None, 'tp')
- norm_gain_gradient: float32 [1024], P('tp')
- grad_bias: float32 [1024], P('tp')
- grad_proj: float32 [2048, 1024], P('sp', 'tp')
All inputs are finite; a program needn't handle non-finite values.
Results may differ from a plain program's by a relative error of at most 0.0049.
Values may be sent and summed in bfloat16 or wider, within the bound.
A program may use at most 64 MiB of HBM per device.

v0:
```python
import jax
import jax.numpy as jnp
from jax import lax
from jax.sharding import PartitionSpec as P

CONV_CHANNELS = 1024
TAPS = 31


def passed_along(shard, axis, by):
    size = lax.axis_size(axis)
    pairs = [(i, i + by) for i in range(size) if 0 <= i + by < size]
    return lax.ppermute(shard, axis, pairs)


def on_device(
    glu_value, glu_gate, conv_taps, channel_norm_gain, channel_norm_bias, out_proj, out_grad
):
    rows, width = glu_value.shape
    value = glu_value.astype(jnp.float32)
    sig_gate = jax.nn.sigmoid(glu_gate.astype(jnp.float32))
    gated = (value * sig_gate).astype(jnp.bfloat16)
    before = passed_along(gated[rows - (TAPS - 1) :], "sp", 1)
    padded = jnp.concatenate([before, gated], axis=0).astype(jnp.float32)
    conv_output = jnp.zeros((rows, width), jnp.float32)
    for k in range(TAPS):
        conv_output = conv_output + conv_taps[k][None, :] * padded[k : k + rows]
    total, squares = lax.psum(
        (jnp.sum(conv_output, axis=1), jnp.sum(conv_output * conv_output, axis=1)), "tp"
    )
    channel_mean = (total / CONV_CHANNELS)[:, None]
    var = (squares / CONV_CHANNELS)[:, None] - channel_mean * channel_mean
    inverse_deviation = lax.rsqrt(var + 1e-05)
    centered_standardized = (conv_output - channel_mean) * inverse_deviation
    normalized_rows = (
        centered_standardized * channel_norm_gain[None, :] + channel_norm_bias[None, :]
    )
    sig_norm = jax.nn.sigmoid(normalized_rows)
    act = (normalized_rows * sig_norm).astype(jnp.bfloat16)
    grad_act = lax.dot_general(
        out_grad, out_proj, (((1,), (1,)), ((), ())), preferred_element_type=jnp.float32
    )
    grad_proj = lax.psum_scatter(
        lax.dot_general(
            out_grad, act, (((0,), (0,)), ((), ())), preferred_element_type=jnp.float32
        ),
        "sp",
        scatter_dimension=0,
        tiled=True,
    )
    normalized_gradient = grad_act * sig_norm * (1.0 + normalized_rows * (1.0 - sig_norm))
    scaled_rows = normalized_gradient * channel_norm_gain[None, :]
    first_term, second_term = lax.psum(
        (jnp.sum(scaled_rows, axis=1), jnp.sum(scaled_rows * centered_standardized, axis=1)), "tp"
    )
    conv_output_gradient = inverse_deviation * (
        scaled_rows
        - (first_term / CONV_CHANNELS)[:, None]
        - centered_standardized * (second_term / CONV_CHANNELS)[:, None]
    )
    taps_local = jnp.stack(
        [jnp.sum(conv_output_gradient * padded[k : k + rows], axis=0) for k in range(TAPS)], axis=0
    )
    packed = jnp.concatenate(
        [
            taps_local,
            jnp.sum(normalized_gradient * centered_standardized, axis=0)[None, :],
            jnp.sum(normalized_gradient, axis=0)[None, :],
        ],
        axis=0,
    )
    share = lax.psum_scatter(packed, "sp", scatter_dimension=1, tiled=True)
    summed = lax.all_gather(share, "sp", axis=1, tiled=True)
    ahead = passed_along(conv_output_gradient[: TAPS - 1], "sp", -1)
    after = jnp.concatenate([conv_output_gradient, ahead], axis=0)
    grad_gated = jnp.zeros((rows, width), jnp.float32)
    for k in range(TAPS):
        grad_gated = grad_gated + conv_taps[k][None, :] * after[TAPS - 1 - k : TAPS - 1 - k + rows]
    grad_value = (grad_gated * sig_gate).astype(jnp.bfloat16)
    grad_gate = (grad_gated * value * sig_gate * (1.0 - sig_gate)).astype(jnp.bfloat16)
    return (grad_value, grad_gate, summed[:TAPS], summed[TAPS], summed[TAPS + 1], grad_proj)


def solution(mesh):
    return jax.shard_map(
        on_device,
        mesh=mesh,
        in_specs=(
            P("sp", "tp"),
            P("sp", "tp"),
            P(None, "tp"),
            P("tp"),
            P("tp"),
            P("tp", None),
            P("sp", None),
        ),
        out_specs=(P("sp", "tp"), P("sp", "tp"), P(None, "tp"), P("tp"), P("tp"), P("sp", "tp")),
        check_vma=False,
    )
```

profile of v0, /device:TPU:0, one launch (start us, length us, event | category | flops | bytes accessed | tf_op | source)
XLA Modules:
  0.0 184.4 jit_solution(906869488730801096)
XLA Ops:
  7.2 0.0 copy-start
  7.2 0.0 reduce-scatter.7.cloned.1.call-start
  7.2 1.6 fusion.1
  8.9 2.4 %collective-permute-start = (bf16[30,512]{1,0:T(8,128)(2,1)S(1)}, bf16[30,512]{1,0:T(8,128)(2,1)S(1)}, u32[]{:S(2)}, u32[]{:S(2)}) collective-permute-start(bf16[30,512]{1,0:T(8,128)(2,1)S(1)} %slice.450), channel_id=1, source_target_pairs={{0,2},{2,4},{4,6},{6,8},{8,10},{10,12},{12,14},{14,16},{16,18},{18... | collective-permute-start | bytes 92168 | tf_op jit(solution)/shard_map/ppermute | solution.py:13
  11.3 1.1 fusion.101
  12.4 1.0 fusion.102
  13.5 0.0 collective-permute-done
  13.5 0.2 maximum_convert_fusion
  13.6 0.0 copy-start.4
  13.6 0.0 copy-start.5
  13.7 5.7 %multiply_reduce_fusion.33 = (f32[512]{0:T(512)S(1)}, f32[512]{0:T(512)S(1)}, f32[512,512]{1,0:T(8,128)}) fusion(f32[542,512]{1,0:T(8,128)S(1)} %maximum_convert_fusion, f32[512]{0:T(512)S(1)} %bitcast.132, f32[512]{0:T(512)S(1)} %bitcast.134, f32[512]{0:T(512)S(1)} %bitcast.76, f32[512]{0:T(512)S(1)} %bitcast.78, f32[512]{0:T(512)S(1)} %bitcast.80, ...), kind=kLoop, calls=%fused_computation.184 | loop fusion | flops 16776192 | bytes 33622016 | tf_op jit(solution)/shard_map/reduce_sum | solution.py:29
  19.4 5.2 %all-reduce.1 = (f32[512]{0:T(512)S(1)}, f32[512]{0:T(512)S(1)}) all-reduce(f32[512]{0:T(512)S(1)} %get-tuple-element.60, f32[512]{0:T(512)S(1)} %get-tuple-element.59), channel_id=1, replica_groups=mesh['sp'=16,'tp'=2] {'tp'}, use_global_device_ids=true, to_apply=%region_3.0 | all-reduce | flops 1024 | bytes 8192 | tf_op jit(solution)/shard_map/psum | solution.py:28
  24.6 0.0 copy-done
  24.6 0.0 copy-done.4
  24.6 0.0 copy-done.5
  24.6 4.6 %multiply_reduce_fusion = (f32[512]{0:T(512)S(1)}, f32[512]{0:T(512)S(1)}, f32[512]{0:T(512)S(1)}, f32[512]{0:T(512)S(1)}, f32[512,512]{1,0:T(8,128)}) fusion(f32[512,512]{1,0:T(8,128)} %get-tuple-element.70, f32[512]{0:T(512)S(1)} %get-tuple-element.103, f32[512]{0:T(512)S(1)} %get-tuple-element.102, f32[512]{0:T(512)S(1)} %copy-done.4, ...), kind=kOutput, calls=%fused_computation.146 | convolution fusion | flops 1078720512 | bytes 6307840 | tf_op jit(solution)/shard_map/dot_general | solution.py:40
  29.2 4.9 %all-reduce = (f32[512]{0:T(512)S(1)}, f32[512]{0:T(512)S(1)}) all-reduce(f32[512]{0:T(512)S(1)} %get-tuple-element.56, f32[512]{0:T(512)S(1)} %get-tuple-element.57), channel_id=1, replica_groups=mesh['sp'=16,'tp'=2] {'tp'}, use_global_device_ids=true, to_apply=%region_7.0 | all-reduce | flops 1024 | bytes 8192 | tf_op jit(solution)/shard_map/psum | solution.py:53
  34.1 4.2 %multiply_reduce_fusion.1 = (f32[512]{0:T(512)S(1)}, f32[512]{0:T(512)S(1)}, f32[512]{0:T(512)S(1)}, f32[512]{0:T(512)S(1)}, f32[512]{0:T(512)S(1)}, /*index=5*/...) fusion(f32[542,512]{1,0:T(8,128)S(1)} %maximum_convert_fusion, ...), kind=kLoop, calls=%fused_computation.147 | loop fusion | flops 11262976 | bytes 22067200 | tf_op jit(solution)/shard_map/reduce_sum | solution.py:62
  38.3 0.0 copy-start.1
  38.3 1.7 multiply_reduce_fusion.19
  40.0 0.0 copy-done.1
  40.0 0.2 concatenate.11
  40.2 0.8 copy.20
  41.0 0.0 reduce-scatter.7.cloned.1.call-update
  41.1 0.0 reduce-scatter.5.cloned.1.call-start
  41.1 4.6 %convolution_bitcast_fusion = f32[2048,512]{0,1:T(8,128)} fusion(bf16[512,2048]{1,0:T(8,128)(2,1)S(1)} %copy-done, f32[512,512]{1,0:T(8,128)} %get-tuple-element.70, f32[512]{0:T(512)S(1)} %copy-done.5, f32[512]{0:T(512)S(1)} %copy-done.4, f32[512]{0:T(512)S(1)} %get-tuple-element.103, f32[512]{0:T(512)S(1)} %get-tuple-element.102), kind=kOutput, calls=%fused_computation.29 | convolution fusion | flops 1076101120 | bytes 7348224 | tf_op jit(solution)/shard_map/dot_general | solution.py:44
  45.7 0.0 copy-start.2
  45.7 0.0 reduce-scatter.5.cloned.1.call-update
  45.8 1.2 copy-done.2
  47.0 0.0 copy-start.3
  47.0 1.4 collective-permute-start.1
  48.4 1.8 %collective-permute-done.1 = f32[30,512]{1,0:T(8,128)S(1)} collective-permute-done((f32[30,512]{1,0:T(8,128)S(1)}, f32[30,512]{1,0:T(8,128)S(1)}, u32[]{:S(2)}, u32[]{:S(2)}) %collective-permute-start.1) | collective-permute-done | bytes 61472 | tf_op jit(solution)/shard_map/ppermute | solution.py:13
  50.2 7.0 %fusion.4 = (bf16[512,512]{1,0:T(8,128)(2,1)}, f32[512,512]{1,0:T(8,128)S(1)}) fusion(bf16[512,512]{1,0:T(8,128)(2,1)} %param.7, bf16[512,512]{1,0:T(8,128)(2,1)} %param.8, f32[512,512]{1,0:T(8,128)S(1)} %copy-done.2, f32[512]{0:T(512)S(1)} %bitcast.133, f32[30,512]{1,0:T(8,128)S(1)} %collective-permute-done.1, f32[512]{0:T(512)S(1)} %bitcast.135, ...), kind=kLoop, calls=%fused_computation.37 | loop fusion | flops 26476544 | bytes 3794944 | tf_op jit(solution)/shard_map/convert_element_type | solution.py:80
  57.2 0.0 copy-done.3
  57.2 1.1 multiply_convert_fusion.1
  58.3 41.8 %reduce-scatter.7.cloned.1.call-done = f32[32,33]{1,0:T(8,128)} async-done(((f32[512,33]{1,0:T(8,128)}), f32[32,33]{1,0:T(8,128)}) %reduce-scatter.7.cloned.1.call-update) | async-done | bytes 4240
  100.1 20.3 %all_gather.3 = f32[33,512]{0,1:T(8,128)S(1)} all-gather(f32[33,32]{0,1:T(8,128)} %bitcast.136), channel_id=1, replica_groups=mesh['sp'=16,'tp'=2] {'sp'}, dimensions={1}, use_global_device_ids=true | all-gather | bytes 71808 | tf_op jit(solution)/shard_map/all_gather | solution.py:73
  120.4 0.7 copy.18
  121.2 1.0 slice_reduce_fusion
  122.1 53.6 %reduce-scatter.5.cloned.1.call-done = f32[128,512]{0,1:T(8,128)} async-done(((f32[2048,512]{0,1:T(8,128)}), f32[128,512]{0,1:T(8,128)}) %reduce-scatter.5.cloned.1.call-update) | async-done | bytes 262160 | tf_op jit(solution)/shard_map/reduce_scatter | solution.py:43
  175.8 1.8 copy.19
  (4 shorter events, 0.0 us)
Async XLA Ops:
  7.2 17.4 %copy-start = (bf16[512,2048]{1,0:T(8,128)(2,1)S(1)}, bf16[512,2048]{1,0:T(8,128)(2,1)}, u32[]{:S(2)}) copy-start(bf16[512,2048]{1,0:T(8,128)(2,1)} %param.13) | copy-start | bytes 6291460
  7.2 92.9 %reduce-scatter.7.cloned.1.call-start = ((), (), s32[]{:S(2)}) async-start(), calls=%async_computation.3 | async-start | bytes 278528
  8.9 4.6 %collective-permute-start = (bf16[30,512]{1,0:T(8,128)(2,1)S(1)}, bf16[30,512]{1,0:T(8,128)(2,1)S(1)}, u32[]{:S(2)}, u32[]{:S(2)}) collective-permute-start(bf16[30,512]{1,0:T(8,128)(2,1)S(1)} %slice.450), channel_id=1, source_target_pairs={{0,2},{2,4},{4,6},{6,8},{8,10},{10,12},{12,14},{14,16},{16,18},{18... | collective-permute-start | bytes 92168 | tf_op jit(solution)/shard_map/ppermute | solution.py:13
  13.6 11.0 %copy-start.4 = (f32[512]{0:T(512)S(1)}, f32[512]{0:T(512)}, u32[]{:S(2)}) copy-start(f32[512]{0:T(512)} %param.10) | copy-start | bytes 6148
  13.6 11.0 %copy-start.5 = (f32[512]{0:T(512)S(1)}, f32[512]{0:T(512)}, u32[]{:S(2)}) copy-start(f32[512]{0:T(512)} %param.11) | copy-start | bytes 6148
  38.3 1.7 copy-start.1
  41.1 134.7 %reduce-scatter.5.cloned.1.call-start = ((), (), s32[]{:S(2)}) async-start(), calls=%async_computation.2 | async-start | bytes 4456448 | tf_op jit(solution)/shard_map/reduce_scatter | solution.py:43
  45.7 1.2 copy-start.2
  47.0 10.3 %copy-start.3 = (bf16[512,512]{1,0:T(8,128)(2,1)S(1)}, bf16[512,512]{1,0:T(8,128)(2,1)}, u32[]{:S(2)}) copy-start(bf16[512,512]{1,0:T(8,128)(2,1)} %param.8) | copy-start | bytes 1572868
  47.0 3.3 %collective-permute-start.1 = (f32[30,512]{1,0:T(8,128)S(1)}, f32[30,512]{1,0:T(8,128)S(1)}, u32[]{:S(2)}, u32[]{:S(2)}) collective-permute-start(f32[30,512]{1,0:T(8,128)S(1)} %slice.482), channel_id=1, source_target_pairs={{2,0},{4,2},{6,4},{8,6},{10,8},{12,10},{14,12},{16,14},{18,16},{20... | collective-permute-start | bytes 184328 | tf_op jit(solution)/shard_map/ppermute | solution.py:13
Sparse Core Ops, SparseCore 0:
  41.2 58.8 reduce-scatter.6
  103.9 71.7 reduce-scatter.4
where the time goes:
time: 185 us; the launch traced here: 184 us
  waiting for transfers between devices  97.3 us (53%)
  blocking collectives  30.4 us (16%)
  other arithmetic  21.5 us (12%)
  between operations  14.2 us (8%)
  matrix products  9.17 us (5%)
  local copies, waits for them, and re-layouts  7.9 us (4%)
  starting transfers between devices  3.9 us (2%)
    reduce_scatter x1, waiting for transfers between devices, on_device(): lax.psum_scatter(lax.dot_general(out_grad, act, (((0,), (0,)), ((), ())),...  53.6 us
    unnamed x3, waiting for transfers between devices  41.8 us
    all_gather x1, blocking collectives, on_device(): summed = lax.all_gather(share, 'sp', axis=1, tiled=True)  20.3 us
    convert_element_type x1, other arithmetic, on_device(): (grad_gated * value * sig_gate * (1.0 - sig_gate)).astype(jnp.bfloat16)  6.99 us
    reduce_sum x2, other arithmetic, on_device(): jnp.sum(conv_output_gradient * padded[k:k + rows], axis=0)  5.89 us
    reduce_sum x1, other arithmetic, on_device(): jnp.sum(conv_output * conv_output, axis=1)  5.75 us
    psum x1, blocking collectives, on_device(): lax.psum((jnp.sum(conv_output, axis=1), jnp.sum(conv_output * conv_output...  5.19 us
    psum x1, blocking collectives, on_device(): lax.psum((jnp.sum(scaled_rows, axis=1), jnp.sum(scaled_rows * centered_st...  4.91 us
  transfers between devices with their start and end apart: 4, of which 3 were waited for; matrix products, arithmetic and copies ran while one was open for 9% of the time, Pallas kernels for 0%

commit v1 on v0

--- a/solution.py
+++ b/solution.py
@@ -70,7 +70,8 @@
         axis=0,
     )
     share = lax.psum_scatter(packed, "sp", scatter_dimension=1, tiled=True)
-    summed = lax.all_gather(share, "sp", axis=1, tiled=True)
+    parts = lax.all_gather(share, "sp", axis=0, tiled=False)
+    summed = jnp.concatenate(parts, axis=1)
     ahead = passed_along(conv_output_gradient[: TAPS - 1], "sp", -1)
     after = jnp.concatenate([conv_output_gradient, ahead], axis=0)
     grad_gated = jnp.zeros((rows, width), jnp.float32)

time: 185 us -> 185 us (level)
  no operation moved by 1% of the time
where the time goes in v1:
time: 185 us; the launch traced here: 184 us
  waiting for transfers between devices  96.5 us (52%)
  blocking collectives  30.4 us (16%)
  other arithmetic  21.5 us (12%)
  between operations  14.2 us (8%)
  matrix products  9.17 us (5%)
  local copies, waits for them, and re-layouts  8.63 us (5%)
  starting transfers between devices  3.9 us (2%)
    reduce_scatter x1, waiting for transfers between devices, on_device(): lax.psum_scatter(lax.dot_general(out_grad, act, (((0,), (0,)), ((), ())),...  52.9 us
    unnamed x3, waiting for transfers between devices  41.8 us
    all_gather x1, blocking collectives, on_device(): parts = lax.all_gather(share, 'sp', axis=0, tiled=False)  20.3 us
    convert_element_type x1, other arithmetic, on_device(): (grad_gated * value * sig_gate * (1.0 - sig_gate)).astype(jnp.bfloat16)  6.99 us
    reduce_sum x2, other arithmetic, on_device(): jnp.sum(conv_output_gradient * padded[k:k + rows], axis=0)  5.89 us
    reduce_sum x1, other arithmetic, on_device(): jnp.sum(conv_output * conv_output, axis=1)  5.75 us
    psum x1, blocking collectives, on_device(): lax.psum((jnp.sum(conv_output, axis=1), jnp.sum(conv_output * conv_output...  5.19 us
    psum x1, blocking collectives, on_device(): lax.psum((jnp.sum(scaled_rows, axis=1), jnp.sum(scaled_rows * centered_st...  4.92 us
  transfers between devices with their start and end apart: 4, of which 3 were waited for; matrix products, arithmetic and copies ran while one was open for 9% of the time, Pallas kernels for 0%

profile of v1, /device:TPU:0, one launch (start us, length us, event | category | flops | bytes accessed | tf_op | source)
XLA Modules:
  0.0 184.4 jit_solution(194042830766719834)
XLA Ops:
  7.2 0.0 copy-start
  7.2 0.0 reduce-scatter.7.cloned.1.call-start
  7.2 1.6 fusion.1
  8.9 2.4 %collective-permute-start = (bf16[30,512]{1,0:T(8,128)(2,1)S(1)}, bf16[30,512]{1,0:T(8,128)(2,1)S(1)}, u32[]{:S(2)}, u32[]{:S(2)}) collective-permute-start(bf16[30,512]{1,0:T(8,128)(2,1)S(1)} %slice.456), channel_id=1, source_target_pairs={{0,2},{2,4},{4,6},{6,8},{8,10},{10,12},{12,14},{14,16},{16,18},{18... | collective-permute-start | bytes 92168 | tf_op jit(solution)/shard_map/ppermute | solution.py:13
  11.3 1.1 fusion.101
  12.4 1.0 fusion.102
  13.5 0.0 collective-permute-done
  13.5 0.2 maximum_convert_fusion
  13.6 0.0 copy-start.4
  13.6 0.0 copy-start.5
  13.7 5.7 %multiply_reduce_fusion.33 = (f32[512]{0:T(512)S(1)}, f32[512]{0:T(512)S(1)}, f32[512,512]{1,0:T(8,128)}) fusion(f32[542,512]{1,0:T(8,128)S(1)} %maximum_convert_fusion, f32[512]{0:T(512)S(1)} %bitcast.137, f32[512]{0:T(512)S(1)} %bitcast.139, f32[512]{0:T(512)S(1)} %bitcast.81, f32[512]{0:T(512)S(1)} %bitcast.83, f32[512]{0:T(512)S(1)} %bitcast.85, ...), kind=kLoop, calls=%fused_computation.184 | loop fusion | flops 16776192 | bytes 33622016 | tf_op jit(solution)/shard_map/reduce_sum | solution.py:29
  19.4 5.2 %all-reduce.1 = (f32[512]{0:T(512)S(1)}, f32[512]{0:T(512)S(1)}) all-reduce(f32[512]{0:T(512)S(1)} %get-tuple-element.66, f32[512]{0:T(512)S(1)} %get-tuple-element.65), channel_id=1, replica_groups=mesh['sp'=16,'tp'=2] {'tp'}, use_global_device_ids=true, to_apply=%region_3.0 | all-reduce | flops 1024 | bytes 8192 | tf_op jit(solution)/shard_map/psum | solution.py:28
  24.6 0.0 copy-done
  24.6 0.0 copy-done.4
  24.6 0.0 copy-done.5
  24.6 4.6 %multiply_reduce_fusion = (f32[512]{0:T(512)S(1)}, f32[512]{0:T(512)S(1)}, f32[512]{0:T(512)S(1)}, f32[512]{0:T(512)S(1)}, f32[512,512]{1,0:T(8,128)}) fusion(f32[512,512]{1,0:T(8,128)} %get-tuple-element.76, f32[512]{0:T(512)S(1)} %get-tuple-element.109, f32[512]{0:T(512)S(1)} %get-tuple-element.108, f32[512]{0:T(512)S(1)} %copy-done.4, ...), kind=kOutput, calls=%fused_computation.146 | convolution fusion | flops 1078720512 | bytes 6307840 | tf_op jit(solution)/shard_map/dot_general | solution.py:40
  29.2 4.9 %all-reduce = (f32[512]{0:T(512)S(1)}, f32[512]{0:T(512)S(1)}) all-reduce(f32[512]{0:T(512)S(1)} %get-tuple-element.62, f32[512]{0:T(512)S(1)} %get-tuple-element.63), channel_id=1, replica_groups=mesh['sp'=16,'tp'=2] {'tp'}, use_global_device_ids=true, to_apply=%region_7.0 | all-reduce | flops 1024 | bytes 8192 | tf_op jit(solution)/shard_map/psum | solution.py:53
  34.1 4.2 %multiply_reduce_fusion.1 = (f32[512]{0:T(512)S(1)}, f32[512]{0:T(512)S(1)}, f32[512]{0:T(512)S(1)}, f32[512]{0:T(512)S(1)}, f32[512]{0:T(512)S(1)}, /*index=5*/...) fusion(f32[542,512]{1,0:T(8,128)S(1)} %maximum_convert_fusion, ...), kind=kLoop, calls=%fused_computation.147 | loop fusion | flops 11262976 | bytes 22067200 | tf_op jit(solution)/shard_map/reduce_sum | solution.py:62
  38.3 0.0 copy-start.1
  38.3 1.7 multiply_reduce_fusion.19
  40.0 0.0 copy-done.1
  40.0 0.2 concatenate.11
  40.2 0.8 copy.22
  41.0 0.0 reduce-scatter.7.cloned.1.call-update
  41.1 0.0 reduce-scatter.5.cloned.1.call-start
  41.1 4.6 %convolution_bitcast_fusion = f32[2048,512]{0,1:T(8,128)} fusion(bf16[512,2048]{1,0:T(8,128)(2,1)S(1)} %copy-done, f32[512,512]{1,0:T(8,128)} %get-tuple-element.76, f32[512]{0:T(512)S(1)} %copy-done.5, f32[512]{0:T(512)S(1)} %copy-done.4, f32[512]{0:T(512)S(1)} %get-tuple-element.109, f32[512]{0:T(512)S(1)} %get-tuple-element.108), kind=kOutput, calls=%fused_computation.29 | convolution fusion | flops 1076101120 | bytes 7348224 | tf_op jit(solution)/shard_map/dot_general | solution.py:44
  45.7 0.0 copy-start.2
  45.7 0.0 reduce-scatter.5.cloned.1.call-update
  45.8 1.2 copy-done.2
  47.0 0.0 copy-start.3
  47.0 1.4 collective-permute-start.1
  48.4 1.8 %collective-permute-done.1 = f32[30,512]{1,0:T(8,128)S(1)} collective-permute-done((f32[30,512]{1,0:T(8,128)S(1)}, f32[30,512]{1,0:T(8,128)S(1)}, u32[]{:S(2)}, u32[]{:S(2)}) %collective-permute-start.1) | collective-permute-done | bytes 61472 | tf_op jit(solution)/shard_map/ppermute | solution.py:13
  50.2 7.0 %fusion.4 = (bf16[512,512]{1,0:T(8,128)(2,1)}, f32[512,512]{1,0:T(8,128)S(1)}) fusion(bf16[512,512]{1,0:T(8,128)(2,1)} %param.7, bf16[512,512]{1,0:T(8,128)(2,1)} %param.8, f32[512,512]{1,0:T(8,128)S(1)} %copy-done.2, f32[512]{0:T(512)S(1)} %bitcast.138, f32[30,512]{1,0:T(8,128)S(1)} %collective-permute-done.1, f32[512]{0:T(512)S(1)} %bitcast.140, ...), kind=kLoop, calls=%fused_computation.37 | loop fusion | flops 26476544 | bytes 3794944 | tf_op jit(solution)/shard_map/convert_element_type | solution.py:81
  57.2 0.0 copy-done.3
  57.2 1.1 multiply_convert_fusion.1
  58.3 41.8 %reduce-scatter.7.cloned.1.call-done = f32[32,33]{1,0:T(8,128)} async-done(((f32[512,33]{1,0:T(8,128)}), f32[32,33]{1,0:T(8,128)}) %reduce-scatter.7.cloned.1.call-update) | async-done | bytes 4240
  100.1 20.3 %all-gather.1 = f32[16,33,32]{1,2,0:T(8,128)S(1)} all-gather(f32[1,33,32]{1,2,0:T(8,128)} %bitcast.141), channel_id=2, replica_groups=mesh['sp'=16,'tp'=2] {'sp'}, dimensions={0}, use_global_device_ids=true | all-gather | bytes 71808 | tf_op jit(solution)/shard_map/all_gather | solution.py:73
  120.4 0.4 slice_reduce_fusion
  120.8 0.7 squeeze.7
  121.5 0.7 squeeze.6
  122.1 0.7 copy.20
  122.9 52.9 %reduce-scatter.5.cloned.1.call-done = f32[128,512]{0,1:T(8,128)} async-done(((f32[2048,512]{0,1:T(8,128)}), f32[128,512]{0,1:T(8,128)}) %reduce-scatter.5.cloned.1.call-update) | async-done | bytes 262160 | tf_op jit(solution)/shard_map/reduce_scatter | solution.py:43
  175.8 1.8 copy.21
  (4 shorter events, 0.0 us)
Async XLA Ops:
  7.2 17.4 %copy-start = (bf16[512,2048]{1,0:T(8,128)(2,1)S(1)}, bf16[512,2048]{1,0:T(8,128)(2,1)}, u32[]{:S(2)}) copy-start(bf16[512,2048]{1,0:T(8,128)(2,1)} %param.13) | copy-start | bytes 6291460
  7.2 92.9 %reduce-scatter.7.cloned.1.call-start = ((), (), s32[]{:S(2)}) async-start(), calls=%async_computation.3 | async-start | bytes 278528
  8.9 4.6 %collective-permute-start = (bf16[30,512]{1,0:T(8,128)(2,1)S(1)}, bf16[30,512]{1,0:T(8,128)(2,1)S(1)}, u32[]{:S(2)}, u32[]{:S(2)}) collective-permute-start(bf16[30,512]{1,0:T(8,128)(2,1)S(1)} %slice.456), channel_id=1, source_target_pairs={{0,2},{2,4},{4,6},{6,8},{8,10},{10,12},{12,14},{14,16},{16,18},{18... | collective-permute-start | bytes 92168 | tf_op jit(solution)/shard_map/ppermute | solution.py:13
  13.6 11.0 %copy-start.4 = (f32[512]{0:T(512)S(1)}, f32[512]{0:T(512)}, u32[]{:S(2)}) copy-start(f32[512]{0:T(512)} %param.10) | copy-start | bytes 6148
  13.6 11.0 %copy-start.5 = (f32[512]{0:T(512)S(1)}, f32[512]{0:T(512)}, u32[]{:S(2)}) copy-start(f32[512]{0:T(512)} %param.11) | copy-start | bytes 6148
  38.3 1.7 copy-start.1
  41.1 134.7 %reduce-scatter.5.cloned.1.call-start = ((), (), s32[]{:S(2)}) async-start(), calls=%async_computation.2 | async-start | bytes 4456448 | tf_op jit(solution)/shard_map/reduce_scatter | solution.py:43
  45.7 1.2 copy-start.2
  47.0 10.3 %copy-start.3 = (bf16[512,512]{1,0:T(8,128)(2,1)S(1)}, bf16[512,512]{1,0:T(8,128)(2,1)}, u32[]{:S(2)}) copy-start(bf16[512,512]{1,0:T(8,128)(2,1)} %param.8) | copy-start | bytes 1572868
  47.0 3.3 %collective-permute-start.1 = (f32[30,512]{1,0:T(8,128)S(1)}, f32[30,512]{1,0:T(8,128)S(1)}, u32[]{:S(2)}, u32[]{:S(2)}) collective-permute-start(f32[30,512]{1,0:T(8,128)S(1)} %slice.488), channel_id=1, source_target_pairs={{2,0},{4,2},{6,4},{8,6},{10,8},{12,10},{14,12},{16,14},{18,16},{20... | collective-permute-start | bytes 184328 | tf_op jit(solution)/shard_map/ppermute | solution.py:13
Sparse Core Ops, SparseCore 0:
  41.2 58.8 reduce-scatter.6
  103.9 71.7 reduce-scatter.4
